TPU v7x, 512 devices: a 4x2x32 block of a 4x8x32 slice. The times are simulated.
512 devices in a mesh: grp: 2 (over y), sp: 32 (over z), tp: 8 (over x, core).
Axes of the slice: x: 4, y: 2, z: 32, core: 2. Of those that a mesh axis runs over, the one named last changes fastest.
The devices are a block of a 4x8x32 slice.
Arguments:
- stream: bfloat16 [49152, 4096], P(('grp', 'sp'), 'tp'), parts along dimension 0, may hold values from -400 to 400
- in_weight: bfloat16 [2, 1024, 4096], P(None, 'sp', 'tp'), may hold values from -0.09375 to 0.09375
- out_weight: bfloat16 [2, 1024, 4096], P(None, 'sp', 'tp'), may hold values from -0.1875 to 0.1875
- group_mix: bfloat16 [2, 4, 256, 256], replicated, may hold values from -0.375 to 0.375
- pool_gain: float32 [2, 1024], replicated, may hold values from 0.1 to 1.9
- norm_gain: float32 [2, 4096], P(None, 'tp'), may hold values from 0.1 to 1.9
- norm_shift: float32 [2, 4096], P(None, 'tp'), may hold values from -3 to 3
Outputs:
- refined: bfloat16 [49152, 4096], P(('grp', 'sp'), 'tp'), parts along dimension 0
There are 2 independent parts, one for each index of `grp`. A program takes and returns all parts, laid end to end along the dimension named above; an argument that names none is the same for every part. Nothing has to cross between parts.
All inputs are finite; a program needn't handle non-finite values.
Results may differ from a plain program's by a relative error of at most 0.015.
Values may be sent and summed in bfloat16 or wider, within the bound.
No kernel may reach another device: no remote copies, remote signals or barrier semaphores. Data moves between devices by JAX's collectives and lax.ppermute only.
A program may use at most 64 MiB of HBM per device.

v0:
```python
import jax
import jax.numpy as jnp
from jax import lax
from jax.sharding import PartitionSpec as P

D = 4096
GROUPS = 4
GROUP_WIDTH = 256
LAYERS = 2
HALO = 32

epsilon = 1e-05


def shifted(x, axis, distance):
    n = lax.axis_size(axis)
    return lax.ppermute(x, axis, [(i, (i + distance) % n) for i in range(n)])


def swapped(x, axis):
    n = lax.axis_size(axis)
    return lax.ppermute(x, axis, [(i, i ^ 1) for i in range(n)])


def chips():
    n = lax.axis_size("tp")
    return [[core + 2 * i for i in range(n // 2)] for core in range(2)]


def every_other():
    n = lax.axis_size("sp")
    return [[first + 2 * i for i in range(n // 2)] for first in range(2)]


def between_chips(x):
    return lax.all_to_all(
        x, "tp", split_axis=0, concat_axis=0, axis_index_groups=chips(), tiled=True
    )


def ordered(first, second, flip, axis):
    return jnp.where(
        flip,
        jnp.concatenate([second, first], axis=axis),
        jnp.concatenate([first, second], axis=axis),
    )


def delayed(x, rows):
    return jnp.pad(x[: x.shape[0] - rows], ((rows, 0), (0, 0)))


def pooled_windows(hidden, group, positions):
    values = jnp.where(positions >= 0, hidden, 0).astype(jnp.float32)
    running = values
    window_sums = jnp.zeros_like(values)
    for octave in range(GROUPS):
        running = running + delayed(running, 2**octave)
        window_sums = jnp.where(group == octave, running, window_sums)
    width = jnp.left_shift(2, group)
    counts = jnp.clip(positions + 1, 1, width).astype(jnp.float32)
    return (window_sums / counts - values).astype(jnp.bfloat16)


def chosen(flag, x, y):
    return jnp.where(flag, x, y)


def chip_partial(kept, sent, whole_in):
    def product(rows):
        return jnp.einsum("tc,goc->gto", rows, whole_in, preferred_element_type=jnp.float32)

    arrived = swapped(product(sent).astype(jnp.bfloat16), "tp")
    return (product(kept) + arrived.astype(jnp.float32)).astype(jnp.bfloat16)


def per_device(stream, in_weight, out_weight, group_mix, pool_gain, norm_gain, norm_shift):
    tok_rows, width = stream.shape
    tok_half = tok_rows // 2
    at_sp = lax.axis_index("sp")
    at_tp = lax.axis_index("tp")
    core = at_tp % 2
    lower = core == 0
    group = at_tp // 2
    flip = at_sp % 2 == 1
    alpha = (2.0 * LAYERS) ** 0.25
    shard = in_weight.shape[1]

    first_in = lax.all_gather(
        in_weight[0], "sp", axis=0, axis_index_groups=every_other(), tiled=True
    )
    later = lax.all_gather(
        jnp.concatenate([out_weight[0], in_weight[1], out_weight[1]], axis=1),
        "sp",
        axis=0,
        axis_index_groups=every_other(),
        tiled=True,
    )

    def interleaved(own, others):
        whole = ordered(own.reshape(-1, shard, width), others.reshape(-1, shard, width), flip, 1)
        return whole.reshape(GROUPS, GROUP_WIDTH, width)

    def from_neighbours(own, *more):
        middle = own.shape[0] // 2
        low = shifted(jnp.concatenate([own[:middle], *more], axis=0), "sp", 1)
        high = shifted(own[middle:], "sp", -1)
        others = jnp.concatenate([low[:middle], high], axis=0)
        return interleaved(own, others), low[middle:]

    def from_partner(own):
        return interleaved(own, swapped(own, "sp"))

    whole_in, earlier = from_neighbours(first_in, stream[tok_rows - HALO :])
    extended = jnp.concatenate([earlier, stream], axis=0)
    rows = tok_half + HALO
    kept = chosen(lower, extended[:rows], extended[tok_half:])
    sent = chosen(lower, extended[tok_half:], extended[:rows])
    drop = HALO // 2
    for layer_index in range(LAYERS):
        positions = (
            at_sp * tok_rows
            + core * tok_half
            - HALO
            + layer_index * drop
            + jnp.arange(kept.shape[0], dtype=jnp.int32)
        )[:, None]
        partial = chip_partial(kept, sent, whole_in)
        pieces = between_chips(partial)
        if layer_index == 1:
            whole_out = from_partner(later[:, 2 * width :])
        hidden = pieces.astype(jnp.float32).sum(axis=0).astype(jnp.bfloat16)
        pooled = pooled_windows(hidden, group, positions)[drop:]
        mixed = jnp.dot(
            pooled,
            lax.dynamic_index_in_dim(group_mix[layer_index], group, 0, keepdims=False),
            preferred_element_type=jnp.float32,
        )
        gains = lax.dynamic_slice_in_dim(
            pool_gain[layer_index], group * GROUP_WIDTH, GROUP_WIDTH
        )
        scaled = (mixed * gains[None, :]).astype(jnp.bfloat16)
        if layer_index == 0:
            copies = jnp.broadcast_to(scaled, (lax.axis_size("tp") // 2, *scaled.shape))
            own_rows = between_chips(copies)
            whole_out, _ = from_neighbours(later[:, :width])
        else:
            own_rows = lax.all_gather(
                scaled[None], "tp", axis=0, axis_index_groups=chips(), tiled=True
            )
        other_rows = swapped(own_rows, "tp")

        def layer_sum(everyone, current):
            branch = jnp.einsum(
                "gti,gic->tc", everyone, whole_out, preferred_element_type=jnp.float32
            )
            summed = alpha * current.astype(jnp.float32) + branch
            return summed, jnp.stack(
                [jnp.sum(summed, axis=1), jnp.sum(summed * summed, axis=1)]
            )

        own_sum, own_stats = layer_sum(own_rows, kept[drop:])
        other_sum, other_stats = layer_sum(other_rows, sent[drop:])
        if layer_index == 0:
            next_in = from_partner(later[:, width : 2 * width])
        stats = jnp.stack([chosen(lower, own_stats, other_stats), chosen(lower, other_stats, own_stats)])
        count = lax.axis_size("tp")
        everyones = lax.all_to_all(
            jnp.broadcast_to(stats, (count, *stats.shape)),
            "tp",
            split_axis=0,
            concat_axis=0,
            tiled=True,
        )
        totals = everyones.sum(axis=0)
        own_totals = chosen(lower, totals[0], totals[1])
        other_totals = chosen(lower, totals[1], totals[0])

        def normalised(summed, sums):
            row_mean = sums[0] / D
            row_var = sums[1] / D - row_mean * row_mean
            normed = (summed - row_mean[:, None]) * lax.rsqrt(row_var + epsilon)[:, None]
            return (
                normed * norm_gain[layer_index][None, :] + norm_shift[layer_index][None, :]
            ).astype(jnp.bfloat16)

        kept = normalised(own_sum, own_totals)
        sent = normalised(other_sum, other_totals)
        whole_in = next_in

    return ordered(kept, sent, core == 1, 0)


def solution(mesh):
    in_specs = (
        P(("grp", "sp"), "tp"),
        P(None, "sp", "tp"),
        P(None, "sp", "tp"),
        P(),
        P(),
        P(None, "tp"),
        P(None, "tp"),
    )
    out_specs = P(("grp", "sp"), "tp")

    return jax.shard_map(
        per_device, mesh=mesh, in_specs=in_specs, out_specs=out_specs, check_vma=False
    )
```

profile of v0, /device:TPU:33, one launch (start us, length us, event | category | flops | bytes accessed | tf_op | source)
XLA Modules:
  0.0 288.8 jit_solution(5619712536897858678)
XLA Ops:
  7.4 70.3 %all-gather = bf16[1,512,512]{2,1,0:T(8,128)(2,1)S(1)} all-gather(bf16[1,32,512]{2,1,0:T(8,128)(2,1)S(1)} %get-tuple-element.32), channel_id=2, replica_groups={{0,16,32,48,64,80,96,112,128,144,160,176,192,208,224,240},{8,24,40,56,7..., dimensions={1}, use_global_device_ids=true | all-gather | bytes 557056 | tf_op jit(solution)/shard_map/all_gather | solution.py:89
  77.8 4.7 %collective-permute-start = (bf16[288,512]{1,0:T(8,128)(2,1)S(1)}, bf16[288,512]{1,0:T(8,128)(2,1)S(1)}, u32[]{:S(2)}, u32[]{:S(2)}) collective-permute-start(bf16[288,512]{1,0:T(8,128)(2,1)S(1)} %pad_maximum_fusion.3), channel_id=1, source_target_pairs={{0,8},{8,16},{16,24},{24,32},{32,40},{40,48},{48,56},{56,64},{64,7... | collective-permute-start | bytes 884744 | tf_op jit(solution)/shard_map/ppermute | solution.py:17
  82.5 2.0 collective-permute-start.1
  84.5 2.7 collective-permute-done
  87.4 2.3 collective-permute-done.1
  90.2 1.6 fusion.2
  91.8 9.7 %collective-permute-start.2 = (bf16[4,416,256]{2,1,0:T(8,128)(2,1)}, bf16[4,416,256]{2,1,0:T(8,128)(2,1)}, u32[]{:S(2)}, u32[]{:S(2)}) collective-permute-start(bf16[4,416,256]{2,1,0:T(8,128)(2,1)} %fusion.2), channel_id=1, source_target_pairs={{0,1},{1,0},{2,3},{3,2},{4,5},{5,4},{6,7},{7,6},{8,9},{9,8},{10,11... | collective-permute-start | bytes 2555912 | tf_op jit(solution)/shard_map/ppermute | solution.py:22
  102.3 1.6 collective-permute-done.2
  103.8 2.7 fusion
  106.6 4.8 %all-to-all-start = ((bf16[4,416,256]{2,1,0:T(8,128)(2,1)}), bf16[4,416,256]{2,1,0:T(8,128)(2,1)S(1)}, u32[]{:S(2)}, u32[]{:S(2)}) async-start(bf16[4,416,256]{2,1,0:T(8,128)(2,1)} %fusion), calls=%async_computation | async-start | bytes 1703936 | tf_op jit(solution)/shard_map/all_to_all | solution.py:36
  112.3 11.5 %all-to-all-done = bf16[4,416,256]{2,1,0:T(8,128)(2,1)S(1)} async-done(((bf16[4,416,256]{2,1,0:T(8,128)(2,1)}), bf16[4,416,256]{2,1,0:T(8,128)(2,1)S(1)}, u32[]{:S(2)}, u32[]{:S(2)}) %all-to-all-start) | async-done | bytes 852000 | tf_op jit(solution)/shard_map/all_to_all | solution.py:36
  125.7 3.6 %all-to-all-start.1 = ((bf16[4,400,256]{2,1,0:T(8,128)(2,1)}), bf16[4,400,256]{2,1,0:T(8,128)(2,1)S(1)}, u32[]{:S(2)}, u32[]{:S(2)}) async-start(bf16[4,400,256]{2,1,0:T(8,128)(2,1)} %broadcast_in_dim.57), calls=%async_computation.1 | async-start | bytes 1638400 | tf_op jit(solution)/shard_map/all_to_all | solution.py:36
  129.3 11.1 %all-to-all-done.1 = bf16[4,400,256]{2,1,0:T(8,128)(2,1)S(1)} async-done(((bf16[4,400,256]{2,1,0:T(8,128)(2,1)}), bf16[4,400,256]{2,1,0:T(8,128)(2,1)S(1)}, u32[]{:S(2)}, u32[]{:S(2)}) %all-to-all-start.1) | async-done | bytes 819232 | tf_op jit(solution)/shard_map/all_to_all | solution.py:36
  140.4 4.3 %collective-permute-start.3 = (bf16[4,400,256]{2,1,0:T(8,128)(2,1)S(1)}, bf16[4,400,256]{2,1,0:T(8,128)(2,1)}, u32[]{:S(2)}, u32[]{:S(2)}) collective-permute-start(bf16[4,400,256]{2,1,0:T(8,128)(2,1)S(1)} %all-to-all-done.1), channel_id=1, source_target_pairs={{0,1},{1,0},{2,3},{3,2},{4,5},{5,4},{6,7},{7,6},{8,9},{9,8},{10,11... | collective-permute-start | bytes 2457608 | tf_op jit(solution)/shard_map/ppermute | solution.py:22
  144.7 34.3 %all-gather.4.cloned.1.call-done = bf16[512,1536]{1,0:T(8,128)(2,1)} async-done(((bf16[32,1536]{1,0:T(8,128)(2,1)}), bf16[512,1536]{1,0:T(8,128)(2,1)}) %all-gather.4.cloned.1.call-update) | async-done | bytes 1572880 | tf_op jit(solution)/shard_map/all_gather | solution.py:92
  180.1 2.0 collective-permute-start.4
  182.1 4.6 %collective-permute-start.5 = (bf16[256,512]{1,0:T(8,128)(2,1)S(1)}, bf16[256,512]{1,0:T(8,128)(2,1)S(1)}, u32[]{:S(2)}, u32[]{:S(2)}) collective-permute-start(bf16[256,512]{1,0:T(8,128)(2,1)S(1)} %get-tuple-element.25), channel_id=1, source_target_pairs={{0,248},{8,0},{16,8},{24,16},{32,24},{40,32},{48,40},{56,48},{64,5... | collective-permute-start | bytes 786440 | tf_op jit(solution)/shard_map/ppermute | solution.py:17
  191.3 1.9 fusion.39
  193.8 16.0 %all-to-all-start.2 = ((f32[8,2,2,400]{3,2,1,0:T(2,128)}), f32[8,2,2,400]{3,2,1,0:T(2,128)S(1)}, u32[]{:S(2)}, u32[]{:S(2)}) async-start(f32[8,2,2,400]{3,2,1,0:T(2,128)} %broadcast_in_dim.58), calls=%async_computation.2 | async-start | bytes 131072 | tf_op jit(solution)/shard_map/all_to_all | solution.py:168
  209.8 2.7 collective-permute-start.6
  212.5 2.2 all-to-all-done.2
  215.1 10.1 %collective-permute-done.6 = bf16[512,512]{1,0:T(8,128)(2,1)S(1)} collective-permute-done((bf16[512,512]{1,0:T(8,128)(2,1)S(1)}, bf16[512,512]{1,0:T(8,128)(2,1)S(1)}, u32[]{:S(2)}, u32[]{:S(2)}) %collective-permute-start.6) | collective-permute-done | bytes 524320 | tf_op jit(solution)/shard_map/ppermute | solution.py:22
  226.4 2.8 collective-permute-start.7
  229.2 1.9 collective-permute-done.7
  231.1 1.5 fusion.1
  232.7 4.1 %all-to-all-start.3 = ((bf16[4,400,256]{2,1,0:T(8,128)(2,1)}), bf16[4,400,256]{2,1,0:T(8,128)(2,1)S(1)}, u32[]{:S(2)}, u32[]{:S(2)}) async-start(bf16[4,400,256]{2,1,0:T(8,128)(2,1)} %fusion.1), calls=%async_computation.3 | async-start | bytes 1638400 | tf_op jit(solution)/shard_map/all_to_all | solution.py:36
  236.9 2.7 collective-permute-start.9
  239.6 9.3 %all-to-all-done.3 = bf16[4,400,256]{2,1,0:T(8,128)(2,1)S(1)} async-done(((bf16[4,400,256]{2,1,0:T(8,128)(2,1)}), bf16[4,400,256]{2,1,0:T(8,128)(2,1)S(1)}, u32[]{:S(2)}, u32[]{:S(2)}) %all-to-all-start.3) | async-done | bytes 819232 | tf_op jit(solution)/shard_map/all_to_all | solution.py:36
  250.7 11.6 %all-gather.1 = bf16[1536,256]{1,0:T(8,128)(2,1)S(1)} all-gather(bf16[384,256]{1,0:T(8,128)(2,1)S(1)} %fusion.9), channel_id=3, replica_groups={{0,2,4,6},{1,3,5,7},{8,10,12,14},{9,11,13,15},{16,18,20,22},{17,19,21,2..., dimensions={0}, use_global_device_ids=true | all-gather | bytes 983040 | tf_op jit(solution)/shard_map/all_gather | solution.py:148
  262.2 6.3 %collective-permute-start.8 = (bf16[4,384,256]{2,1,0:T(8,128)(2,1)S(1)}, bf16[4,384,256]{2,1,0:T(8,128)(2,1)S(1)}, u32[]{:S(2)}, u32[]{:S(2)}) collective-permute-start(bf16[4,384,256]{2,1,0:T(8,128)(2,1)S(1)} %bitcast.121), channel_id=1, source_target_pairs={{0,1},{1,0},{2,3},{3,2},{4,5},{5,4},{6,7},{7,6},{8,9},{9,8},{10,11... | collective-permute-start | bytes 2359304 | tf_op jit(solution)/shard_map/ppermute | solution.py:22
  271.8 3.6 %all-to-all-start.4 = ((f32[8,2,2,384]{3,2,1,0:T(2,128)}), f32[8,2,2,384]{3,2,1,0:T(2,128)S(1)}, u32[]{:S(2)}, u32[]{:S(2)}) async-start(f32[8,2,2,384]{3,2,1,0:T(2,128)} %broadcast_in_dim.63), calls=%async_computation.4 | async-start | bytes 98304 | tf_op jit(solution)/shard_map/all_to_all | solution.py:168
  275.5 4.8 %all-to-all-done.4 = f32[8,2,2,384]{3,2,1,0:T(2,128)S(1)} async-done(((f32[8,2,2,384]{3,2,1,0:T(2,128)}), f32[8,2,2,384]{3,2,1,0:T(2,128)S(1)}, u32[]{:S(2)}, u32[]{:S(2)}) %all-to-all-start.4) | async-done | bytes 49184 | tf_op jit(solution)/shard_map/all_to_all | solution.py:168
  (104 shorter events, 19.6 us)
Async XLA Ops:
  6.5 71.2 %slice-start = ((bf16[768,512]{1,0:T(8,128)(2,1)}), bf16[32,512]{1,0:T(8,128)(2,1)S(1)}, s32[]{:S(2)}) async-start(bf16[768,512]{1,0:T(8,128)(2,1)} %param.7), calls=%async_computation.6 | async-start | bytes 65536 | tf_op jit(solution)/shard_map/slice | solution.py:114
  6.5 80.7 %copy-start = (bf16[768,512]{1,0:T(8,128)(2,1)S(1)}, bf16[768,512]{1,0:T(8,128)(2,1)}, u32[]{:S(2)}) copy-start(bf16[768,512]{1,0:T(8,128)(2,1)} %param.7) | copy-start | bytes 2359300
  6.6 172.5 %all-gather.4.cloned.1.call-start = ((), (), s32[]{:S(2)}) async-start(), calls=%async_computation.5 | async-start | bytes 1671168 | tf_op jit(solution)/shard_map/all_gather | solution.py:92
  77.8 9.4 %collective-permute-start = (bf16[288,512]{1,0:T(8,128)(2,1)S(1)}, bf16[288,512]{1,0:T(8,128)(2,1)S(1)}, u32[]{:S(2)}, u32[]{:S(2)}) collective-permute-start(bf16[288,512]{1,0:T(8,128)(2,1)S(1)} %pad_maximum_fusion.3), channel_id=1, source_target_pairs={{0,8},{8,16},{16,24},{24,32},{32,40},{40,48},{48,56},{56,64},{64,7... | collective-permute-start | bytes 884744 | tf_op jit(solution)/shard_map/ppermute | solution.py:17
  82.5 7.1 %collective-permute-start.1 = (bf16[256,512]{1,0:T(8,128)(2,1)S(1)}, bf16[256,512]{1,0:T(8,128)(2,1)S(1)}, u32[]{:S(2)}, u32[]{:S(2)}) collective-permute-start(bf16[256,512]{1,0:T(8,128)(2,1)S(1)} %get-tuple-element.31), channel_id=1, source_target_pairs={{0,248},{8,0},{16,8},{24,16},{32,24},{40,32},{48,40},{56,48},{64,5... | collective-permute-start | bytes 786440 | tf_op jit(solution)/shard_map/ppermute | solution.py:17
  87.4 16.5 %copy-start.2 = (bf16[416,512]{1,0:T(8,128)(2,1)}, bf16[416,512]{1,0:T(8,128)(2,1)S(1)}, u32[]{:S(2)}) copy-start(bf16[416,512]{1,0:T(8,128)(2,1)S(1)} %get-tuple-element.28) | copy-start | bytes 1277956
  90.2 11.3 %copy-start.8 = (bf16[2,32,512]{2,1,0:T(8,128)(2,1)S(1)}, bf16[2,32,512]{2,1,0:T(8,128)(2,1)}, u32[]{:S(2)}) copy-start(bf16[2,32,512]{2,1,0:T(8,128)(2,1)} %param.9) | copy-start | bytes 196612
  91.8 12.0 %collective-permute-start.2 = (bf16[4,416,256]{2,1,0:T(8,128)(2,1)}, bf16[4,416,256]{2,1,0:T(8,128)(2,1)}, u32[]{:S(2)}, u32[]{:S(2)}) collective-permute-start(bf16[4,416,256]{2,1,0:T(8,128)(2,1)} %fusion.2), channel_id=1, source_target_pairs={{0,1},{1,0},{2,3},{3,2},{4,5},{5,4},{6,7},{7,6},{8,9},{9,8},{10,11... | collective-permute-start | bytes 2555912 | tf_op jit(solution)/shard_map/ppermute | solution.py:22
  106.6 4.8 %copy-start.9 = (f32[2,1024]{1,0:T(2,128)S(1)}, f32[2,1024]{1,0:T(2,128)}, u32[]{:S(2)}) copy-start(f32[2,1024]{1,0:T(2,128)} %param.11) | copy-start | bytes 24580
  106.6 4.9 %copy-start.1 = (bf16[2,4,256,256]{3,2,1,0:T(8,128)(2,1)S(1)}, bf16[2,4,256,256]{3,2,1,0:T(8,128)(2,1)}, u32[]{:S(2)}) copy-start(bf16[2,4,256,256]{3,2,1,0:T(8,128)(2,1)} %param.10) | copy-start | bytes 3145732
  106.6 17.2 %all-to-all-start = ((bf16[4,416,256]{2,1,0:T(8,128)(2,1)}), bf16[4,416,256]{2,1,0:T(8,128)(2,1)S(1)}, u32[]{:S(2)}, u32[]{:S(2)}) async-start(bf16[4,416,256]{2,1,0:T(8,128)(2,1)} %fusion), calls=%async_computation | async-start | bytes 1703936 | tf_op jit(solution)/shard_map/all_to_all | solution.py:36
  124.7 4.6 %copy-start.10 = (f32[2,512]{1,0:T(2,128)S(1)}, f32[2,512]{1,0:T(2,128)}, u32[]{:S(2)}) copy-start(f32[2,512]{1,0:T(2,128)} %param.12) | copy-start | bytes 12292
  125.7 14.7 %all-to-all-start.1 = ((bf16[4,400,256]{2,1,0:T(8,128)(2,1)}), bf16[4,400,256]{2,1,0:T(8,128)(2,1)S(1)}, u32[]{:S(2)}, u32[]{:S(2)}) async-start(bf16[4,400,256]{2,1,0:T(8,128)(2,1)} %broadcast_in_dim.57), calls=%async_computation.1 | async-start | bytes 1638400 | tf_op jit(solution)/shard_map/all_to_all | solution.py:36
  140.4 50.9 %collective-permute-start.3 = (bf16[4,400,256]{2,1,0:T(8,128)(2,1)S(1)}, bf16[4,400,256]{2,1,0:T(8,128)(2,1)}, u32[]{:S(2)}, u32[]{:S(2)}) collective-permute-start(bf16[4,400,256]{2,1,0:T(8,128)(2,1)S(1)} %all-to-all-done.1), channel_id=1, source_target_pairs={{0,1},{1,0},{2,3},{3,2},{4,5},{5,4},{6,7},{7,6},{8,9},{9,8},{10,11... | collective-permute-start | bytes 2457608 | tf_op jit(solution)/shard_map/ppermute | solution.py:22
  180.1 8.8 %collective-permute-start.4 = (bf16[256,512]{1,0:T(8,128)(2,1)S(1)}, bf16[256,512]{1,0:T(8,128)(2,1)S(1)}, u32[]{:S(2)}, u32[]{:S(2)}) collective-permute-start(bf16[256,512]{1,0:T(8,128)(2,1)S(1)} %get-tuple-element.24), channel_id=1, source_target_pairs={{0,8},{8,16},{16,24},{24,32},{32,40},{40,48},{48,56},{56,64},{64,7... | collective-permute-start | bytes 786440 | tf_op jit(solution)/shard_map/ppermute | solution.py:17
  182.1 7.9 %collective-permute-start.5 = (bf16[256,512]{1,0:T(8,128)(2,1)S(1)}, bf16[256,512]{1,0:T(8,128)(2,1)S(1)}, u32[]{:S(2)}, u32[]{:S(2)}) collective-permute-start(bf16[256,512]{1,0:T(8,128)(2,1)S(1)} %get-tuple-element.25), channel_id=1, source_target_pairs={{0,248},{8,0},{16,8},{24,16},{32,24},{40,32},{48,40},{56,48},{64,5... | collective-permute-start | bytes 786440 | tf_op jit(solution)/shard_map/ppermute | solution.py:17
  188.2 2.3 copy-start.3
  191.3 18.6 %copy-start.11 = (f32[2,512]{1,0:T(2,128)S(1)}, f32[2,512]{1,0:T(2,128)}, u32[]{:S(2)}) copy-start(f32[2,512]{1,0:T(2,128)} %param.13) | copy-start | bytes 12292
  193.8 20.8 %all-to-all-start.2 = ((f32[8,2,2,400]{3,2,1,0:T(2,128)}), f32[8,2,2,400]{3,2,1,0:T(2,128)S(1)}, u32[]{:S(2)}, u32[]{:S(2)}) async-start(f32[8,2,2,400]{3,2,1,0:T(2,128)} %broadcast_in_dim.58), calls=%async_computation.2 | async-start | bytes 131072 | tf_op jit(solution)/shard_map/all_to_all | solution.py:168
  209.8 15.4 %collective-permute-start.6 = (bf16[512,512]{1,0:T(8,128)(2,1)S(1)}, bf16[512,512]{1,0:T(8,128)(2,1)S(1)}, u32[]{:S(2)}, u32[]{:S(2)}) collective-permute-start(bf16[512,512]{1,0:T(8,128)(2,1)S(1)} %get-tuple-element.22), channel_id=1, source_target_pairs={{0,8},{8,0},{16,24},{24,16},{32,40},{40,32},{48,56},{56,48},{64,72... | collective-permute-start | bytes 1572872 | tf_op jit(solution)/shard_map/ppermute | solution.py:22
  215.1 11.3 %copy-start.4 = (bf16[400,512]{1,0:T(8,128)(2,1)}, bf16[400,512]{1,0:T(8,128)(2,1)S(1)}, u32[]{:S(2)}) copy-start(bf16[400,512]{1,0:T(8,128)(2,1)S(1)} %get-tuple-element.53) | copy-start | bytes 1228804
  215.1 16.0 %copy-start.6 = (bf16[400,512]{1,0:T(8,128)(2,1)}, bf16[400,512]{1,0:T(8,128)(2,1)S(1)}, u32[]{:S(2)}) copy-start(bf16[400,512]{1,0:T(8,128)(2,1)S(1)} %get-tuple-element.52) | copy-start | bytes 1228804
  226.4 4.8 %collective-permute-start.7 = (bf16[4,400,256]{2,1,0:T(8,128)(2,1)S(1)}, bf16[4,400,256]{2,1,0:T(8,128)(2,1)S(1)}, u32[]{:S(2)}, u32[]{:S(2)}) collective-permute-start(bf16[4,400,256]{2,1,0:T(8,128)(2,1)S(1)} %fusion.3), channel_id=1, source_target_pairs={{0,1},{1,0},{2,3},{3,2},{4,5},{5,4},{6,7},{7,6},{8,9},{9,8},{10,11... | collective-permute-start | bytes 2457608 | tf_op jit(solution)/shard_map/ppermute | solution.py:22
  232.7 16.2 %all-to-all-start.3 = ((bf16[4,400,256]{2,1,0:T(8,128)(2,1)}), bf16[4,400,256]{2,1,0:T(8,128)(2,1)S(1)}, u32[]{:S(2)}, u32[]{:S(2)}) async-start(bf16[4,400,256]{2,1,0:T(8,128)(2,1)} %fusion.1), calls=%async_computation.3 | async-start | bytes 1638400 | tf_op jit(solution)/shard_map/all_to_all | solution.py:36
  236.9 31.7 %collective-permute-start.9 = (bf16[512,512]{1,0:T(8,128)(2,1)S(1)}, bf16[512,512]{1,0:T(8,128)(2,1)S(1)}, u32[]{:S(2)}, u32[]{:S(2)}) collective-permute-start(bf16[512,512]{1,0:T(8,128)(2,1)S(1)} %get-tuple-element.21), channel_id=1, source_target_pairs={{0,8},{8,0},{16,24},{24,16},{32,40},{40,32},{48,56},{56,48},{64,72... | collective-permute-start | bytes 1572872 | tf_op jit(solution)/shard_map/ppermute | solution.py:22
  250.7 18.4 %copy-start.7 = (bf16[400,512]{1,0:T(8,128)(2,1)S(1)}, bf16[400,512]{1,0:T(8,128)(2,1)}, u32[]{:S(2)}) copy-start(bf16[400,512]{1,0:T(8,128)(2,1)} %copy-done.6) | copy-start | bytes 1228804
  262.2 8.2 %collective-permute-start.8 = (bf16[4,384,256]{2,1,0:T(8,128)(2,1)S(1)}, bf16[4,384,256]{2,1,0:T(8,128)(2,1)S(1)}, u32[]{:S(2)}, u32[]{:S(2)}) collective-permute-start(bf16[4,384,256]{2,1,0:T(8,128)(2,1)S(1)} %bitcast.121), channel_id=1, source_target_pairs={{0,1},{1,0},{2,3},{3,2},{4,5},{5,4},{6,7},{7,6},{8,9},{9,8},{10,11... | collective-permute-start | bytes 2359304 | tf_op jit(solution)/shard_map/ppermute | solution.py:22
  269.1 1.4 copy-start.5
  271.8 8.5 %all-to-all-start.4 = ((f32[8,2,2,384]{3,2,1,0:T(2,128)}), f32[8,2,2,384]{3,2,1,0:T(2,128)S(1)}, u32[]{:S(2)}, u32[]{:S(2)}) async-start(f32[8,2,2,384]{3,2,1,0:T(2,128)} %broadcast_in_dim.63), calls=%async_computation.4 | async-start | bytes 98304 | tf_op jit(solution)/shard_map/all_to_all | solution.py:168
Sparse Core Ops, SparseCore 0:
  102.4 76.6 all-gather.3
where the time goes:
time: 290 us; the launch traced here: 289 us
  waiting for transfers between devices  94.2 us (32%)
  blocking collectives  81.9 us (28%)
  starting transfers between devices  73.8 us (25%)
  between operations  14 us (5%)
  matrix products  11.9 us (4%)
  local copies, waits for them, and re-layouts  6.86 us (2%)
  other arithmetic  6.05 us (2%)
    all_gather x1, blocking collectives, per_device(): lax.all_gather(in_weight[0], 'sp', axis=0, axis_index_groups=every_other(...  70.3 us
    all_gather x1, waiting for transfers between devices, per_device(): lax.all_gather(jnp.concatenate([out_weight[0], in_weight[1], out_weight[1...  34.3 us
    all_to_all x3, waiting for transfers between devices, between_chips(): lax.all_to_all(x, 'tp', split_axis=0, concat_axis=0, axis_index_groups=ch...  31.9 us
    ppermute x6, starting transfers between devices, swapped(): return lax.ppermute(x, axis, [(i, i ^ 1) for i in range(n)])  28.5 us
    all_to_all x2, starting transfers between devices, per_device(): lax.all_to_all(jnp.broadcast_to(stats, (count, *stats.shape)), 'tp', spli...  19.6 us
    ppermute x6, waiting for transfers between devices, swapped(): return lax.ppermute(x, axis, [(i, i ^ 1) for i in range(n)])  14.3 us
    ppermute x4, starting transfers between devices, shifted(): return lax.ppermute(x, axis, [(i, (i + distance) % n) for i in range(n)])  13.2 us
    all_to_all x3, starting transfers between devices, between_chips(): lax.all_to_all(x, 'tp', split_axis=0, concat_axis=0, axis_index_groups=ch...  12.5 us
  transfers between devices with their start and end apart: 16, of which 14 were waited for; matrix products, arithmetic and copies ran while one was open for 5% of the time, Pallas kernels for 0%

commit v1 on v0

--- a/solution.py
+++ b/solution.py
@@ -90,9 +90,9 @@
         in_weight[0], "sp", axis=0, axis_index_groups=every_other(), tiled=True
     )
     later = lax.all_gather(
-        jnp.concatenate([out_weight[0], in_weight[1], out_weight[1]], axis=1),
+        jnp.concatenate([out_weight, in_weight[1:]], axis=0),
         "sp",
-        axis=0,
+        axis=1,
         axis_index_groups=every_other(),
         tiled=True,
     )
@@ -128,7 +128,7 @@
         partial = chip_partial(kept, sent, whole_in)
         pieces = between_chips(partial)
         if layer_index == 1:
-            whole_out = from_partner(later[:, 2 * width :])
+            whole_out = from_partner(later[1])
         hidden = pieces.astype(jnp.float32).sum(axis=0).astype(jnp.bfloat16)
         pooled = pooled_windows(hidden, group, positions)[drop:]
         mixed = jnp.dot(
@@ -143,7 +143,7 @@
         if layer_index == 0:
             copies = jnp.broadcast_to(scaled, (lax.axis_size("tp") // 2, *scaled.shape))
             own_rows = between_chips(copies)
-            whole_out, _ = from_neighbours(later[:, :width])
+            whole_out, _ = from_neighbours(later[0])
         else:
             own_rows = lax.all_gather(
                 scaled[None], "tp", axis=0, axis_index_groups=chips(), tiled=True
@@ -162,7 +162,7 @@
         own_sum, own_stats = layer_sum(own_rows, kept[drop:])
         other_sum, other_stats = layer_sum(other_rows, sent[drop:])
         if layer_index == 0:
-            next_in = from_partner(later[:, width : 2 * width])
+            next_in = from_partner(later[2])
         stats = jnp.stack([chosen(lower, own_stats, other_stats), chosen(lower, other_stats, own_stats)])
         count = lax.axis_size("tp")
         everyones = lax.all_to_all(
@@ -184,11 +184,12 @@
                 normed * norm_gain[layer_index][None, :] + norm_shift[layer_index][None, :]
             ).astype(jnp.bfloat16)
 
+        if layer_index == LAYERS - 1:
+            sums = ordered(own_sum, other_sum, core == 1, 0)
+            return normalised(sums, jnp.concatenate([totals[0], totals[1]], axis=1))
         kept = normalised(own_sum, own_totals)
         sent = normalised(other_sum, other_totals)
         whole_in = next_in
-
-    return ordered(kept, sent, core == 1, 0)
 
 
 def solution(mesh):

time: 290 us -> 290 us (level)
  transfers between devices with their start and end apart: 16 -> 16, of which waited for: 14 -> 13; matrix products, arithmetic and copies ran while one was open for 5% -> 5% of each run, Pallas kernels for 0% -> 0%
where the time goes in v1:
time: 290 us; the launch traced here: 289 us
  waiting for transfers between devices  92.6 us (32%)
  blocking collectives  81.9 us (28%)
  starting transfers between devices  74.8 us (26%)
  between operations  14 us (5%)
  matrix products  11.9 us (4%)
  local copies, waits for them, and re-layouts  7.94 us (3%)
  other arithmetic  5.76 us (2%)
    all_gather x1, blocking collectives, per_device(): lax.all_gather(in_weight[0], 'sp', axis=0, axis_index_groups=every_other(...  70.3 us
    all_gather x1, waiting for transfers between devices, per_device(): lax.all_gather(jnp.concatenate([out_weight, in_weight[1:]], axis=0), 'sp'...  33.9 us
    all_to_all x3, waiting for transfers between devices, between_chips(): lax.all_to_all(x, 'tp', split_axis=0, concat_axis=0, axis_index_groups=ch...  31.3 us
    ppermute x6, starting transfers between devices, swapped(): return lax.ppermute(x, axis, [(i, i ^ 1) for i in range(n)])  29.6 us
    all_to_all x2, starting transfers between devices, per_device(): lax.all_to_all(jnp.broadcast_to(stats, (count, *stats.shape)), 'tp', spli...  19.3 us
    ppermute x6, waiting for transfers between devices, swapped(): return lax.ppermute(x, axis, [(i, i ^ 1) for i in range(n)])  14.5 us
    ppermute x4, starting transfers between devices, shifted(): return lax.ppermute(x, axis, [(i, (i + distance) % n) for i in range(n)])  13.2 us
    all_to_all x3, starting transfers between devices, between_chips(): lax.all_to_all(x, 'tp', split_axis=0, concat_axis=0, axis_index_groups=ch...  12.6 us
  transfers between devices with their start and end apart: 16, of which 13 were waited for; matrix products, arithmetic and copies ran while one was open for 5% of the time, Pallas kernels for 0%

profile of v1, /device:TPU:33, one launch (start us, length us, event | category | flops | bytes accessed | tf_op | source)
XLA Modules:
  0.0 288.9 jit_solution(4716214034058564308)
XLA Ops:
  7.4 70.3 %all-gather = bf16[1,512,512]{2,1,0:T(8,128)(2,1)S(1)} all-gather(bf16[1,32,512]{2,1,0:T(8,128)(2,1)S(1)} %get-tuple-element.32), channel_id=2, replica_groups={{0,16,32,48,64,80,96,112,128,144,160,176,192,208,224,240},{8,24,40,56,7..., dimensions={1}, use_global_device_ids=true | all-gather | bytes 557056 | tf_op jit(solution)/shard_map/all_gather | solution.py:89
  77.8 4.7 %collective-permute-start = (bf16[288,512]{1,0:T(8,128)(2,1)S(1)}, bf16[288,512]{1,0:T(8,128)(2,1)S(1)}, u32[]{:S(2)}, u32[]{:S(2)}) collective-permute-start(bf16[288,512]{1,0:T(8,128)(2,1)S(1)} %pad_maximum_fusion.3), channel_id=1, source_target_pairs={{0,8},{8,16},{16,24},{24,32},{32,40},{40,48},{48,56},{56,64},{64,7... | collective-permute-start | bytes 884744 | tf_op jit(solution)/shard_map/ppermute | solution.py:17
  82.5 2.0 collective-permute-start.1
  84.5 2.7 collective-permute-done
  87.4 2.3 collective-permute-done.1
  91.8 9.7 %collective-permute-start.2 = (bf16[4,416,256]{2,1,0:T(8,128)(2,1)}, bf16[4,416,256]{2,1,0:T(8,128)(2,1)}, u32[]{:S(2)}, u32[]{:S(2)}) collective-permute-start(bf16[4,416,256]{2,1,0:T(8,128)(2,1)} %fusion.7), channel_id=1, source_target_pairs={{0,1},{1,0},{2,3},{3,2},{4,5},{5,4},{6,7},{7,6},{8,9},{9,8},{10,11... | collective-permute-start | bytes 2555912 | tf_op jit(solution)/shard_map/ppermute | solution.py:22
  102.3 1.6 collective-permute-done.2
  103.8 2.7 fusion
  106.5 4.8 %all-to-all-start = ((bf16[4,416,256]{2,1,0:T(8,128)(2,1)}), bf16[4,416,256]{2,1,0:T(8,128)(2,1)S(1)}, u32[]{:S(2)}, u32[]{:S(2)}) async-start(bf16[4,416,256]{2,1,0:T(8,128)(2,1)} %fusion), calls=%async_computation | async-start | bytes 1703936 | tf_op jit(solution)/shard_map/all_to_all | solution.py:36
  112.3 11.4 %all-to-all-done = bf16[4,416,256]{2,1,0:T(8,128)(2,1)S(1)} async-done(((bf16[4,416,256]{2,1,0:T(8,128)(2,1)}), bf16[4,416,256]{2,1,0:T(8,128)(2,1)S(1)}, u32[]{:S(2)}, u32[]{:S(2)}) %all-to-all-start) | async-done | bytes 852000 | tf_op jit(solution)/shard_map/all_to_all | solution.py:36
  125.6 3.6 %all-to-all-start.1 = ((bf16[4,400,256]{2,1,0:T(8,128)(2,1)}), bf16[4,400,256]{2,1,0:T(8,128)(2,1)S(1)}, u32[]{:S(2)}, u32[]{:S(2)}) async-start(bf16[4,400,256]{2,1,0:T(8,128)(2,1)} %broadcast_in_dim.55), calls=%async_computation.1 | async-start | bytes 1638400 | tf_op jit(solution)/shard_map/all_to_all | solution.py:36
  129.2 11.1 %all-to-all-done.1 = bf16[4,400,256]{2,1,0:T(8,128)(2,1)S(1)} async-done(((bf16[4,400,256]{2,1,0:T(8,128)(2,1)}), bf16[4,400,256]{2,1,0:T(8,128)(2,1)S(1)}, u32[]{:S(2)}, u32[]{:S(2)}) %all-to-all-start.1) | async-done | bytes 819232 | tf_op jit(solution)/shard_map/all_to_all | solution.py:36
  140.4 4.3 %collective-permute-start.3 = (bf16[4,400,256]{2,1,0:T(8,128)(2,1)S(1)}, bf16[4,400,256]{2,1,0:T(8,128)(2,1)}, u32[]{:S(2)}, u32[]{:S(2)}) collective-permute-start(bf16[4,400,256]{2,1,0:T(8,128)(2,1)S(1)} %all-to-all-done.1), channel_id=1, source_target_pairs={{0,1},{1,0},{2,3},{3,2},{4,5},{5,4},{6,7},{7,6},{8,9},{9,8},{10,11... | collective-permute-start | bytes 2457608 | tf_op jit(solution)/shard_map/ppermute | solution.py:22
  144.7 33.9 %all-gather.4.cloned.1.call-done = bf16[3,512,512]{2,1,0:T(8,128)(2,1)} async-done(((bf16[3,32,512]{2,1,0:T(8,128)(2,1)}), bf16[3,512,512]{2,1,0:T(8,128)(2,1)}) %all-gather.4.cloned.1.call-update) | async-done | bytes 1572880 | tf_op jit(solution)/shard_map/all_gather | solution.py:92
  179.6 2.5 collective-permute-start.4
  182.1 4.1 %collective-permute-start.5 = (bf16[256,512]{1,0:T(8,128)(2,1)S(1)}, bf16[256,512]{1,0:T(8,128)(2,1)S(1)}, u32[]{:S(2)}, u32[]{:S(2)}) collective-permute-start(bf16[256,512]{1,0:T(8,128)(2,1)S(1)} %get-tuple-element.25), channel_id=1, source_target_pairs={{0,248},{8,0},{16,8},{24,16},{32,24},{40,32},{48,40},{56,48},{64,5... | collective-permute-start | bytes 786440 | tf_op jit(solution)/shard_map/ppermute | solution.py:17
  186.2 2.6 slice_bitcast_fusion.6
  188.8 1.6 collective-permute-done.5
  191.7 1.9 fusion.43
  194.2 15.7 %all-to-all-start.2 = ((f32[8,2,2,400]{3,2,1,0:T(2,128)}), f32[8,2,2,400]{3,2,1,0:T(2,128)S(1)}, u32[]{:S(2)}, u32[]{:S(2)}) async-start(f32[8,2,2,400]{3,2,1,0:T(2,128)} %broadcast_in_dim.56), calls=%async_computation.2 | async-start | bytes 131072 | tf_op jit(solution)/shard_map/all_to_all | solution.py:168
  209.9 3.3 %collective-permute-start.6 = (bf16[512,512]{1,0:T(8,128)(2,1)}, bf16[512,512]{1,0:T(8,128)(2,1)S(1)}, u32[]{:S(2)}, u32[]{:S(2)}) collective-permute-start(bf16[512,512]{1,0:T(8,128)(2,1)} %get-tuple-element.20), channel_id=1, source_target_pairs={{0,8},{8,0},{16,24},{24,16},{32,40},{40,32},{48,56},{56,48},{64,72... | collective-permute-start | bytes 1572872 | tf_op jit(solution)/shard_map/ppermute | solution.py:22
  213.2 1.6 all-to-all-done.2
  215.2 10.3 %collective-permute-done.6 = bf16[512,512]{1,0:T(8,128)(2,1)S(1)} collective-permute-done((bf16[512,512]{1,0:T(8,128)(2,1)}, bf16[512,512]{1,0:T(8,128)(2,1)S(1)}, u32[]{:S(2)}, u32[]{:S(2)}) %collective-permute-start.6) | collective-permute-done | bytes 524320 | tf_op jit(solution)/shard_map/ppermute | solution.py:22
  226.6 2.8 collective-permute-start.7
  229.5 1.9 collective-permute-done.7
  232.9 4.3 %all-to-all-start.3 = ((bf16[4,400,256]{2,1,0:T(8,128)(2,1)}), bf16[4,400,256]{2,1,0:T(8,128)(2,1)S(1)}, u32[]{:S(2)}, u32[]{:S(2)}) async-start(bf16[4,400,256]{2,1,0:T(8,128)(2,1)} %fusion.1), calls=%async_computation.3 | async-start | bytes 1638400 | tf_op jit(solution)/shard_map/all_to_all | solution.py:36
  237.3 3.3 %collective-permute-start.9 = (bf16[512,512]{1,0:T(8,128)(2,1)S(1)}, bf16[512,512]{1,0:T(8,128)(2,1)S(1)}, u32[]{:S(2)}, u32[]{:S(2)}) collective-permute-start(bf16[512,512]{1,0:T(8,128)(2,1)S(1)} %copy-done.2), channel_id=1, source_target_pairs={{0,8},{8,0},{16,24},{24,16},{32,40},{40,32},{48,56},{56,48},{64,72... | collective-permute-start | bytes 1572872 | tf_op jit(solution)/shard_map/ppermute | solution.py:22
  240.6 8.7 %all-to-all-done.3 = bf16[4,400,256]{2,1,0:T(8,128)(2,1)S(1)} async-done(((bf16[4,400,256]{2,1,0:T(8,128)(2,1)}), bf16[4,400,256]{2,1,0:T(8,128)(2,1)S(1)}, u32[]{:S(2)}, u32[]{:S(2)}) %all-to-all-start.3) | async-done | bytes 819232 | tf_op jit(solution)/shard_map/all_to_all | solution.py:36
  251.1 11.6 %all-gather.1 = bf16[1536,256]{1,0:T(8,128)(2,1)S(1)} all-gather(bf16[384,256]{1,0:T(8,128)(2,1)S(1)} %fusion.14), channel_id=3, replica_groups={{0,2,4,6},{1,3,5,7},{8,10,12,14},{9,11,13,15},{16,18,20,22},{17,19,21,2..., dimensions={0}, use_global_device_ids=true | all-gather | bytes 983040 | tf_op jit(solution)/shard_map/all_gather | solution.py:148
  262.7 6.3 %collective-permute-start.8 = (bf16[4,384,256]{2,1,0:T(8,128)(2,1)S(1)}, bf16[4,384,256]{2,1,0:T(8,128)(2,1)S(1)}, u32[]{:S(2)}, u32[]{:S(2)}) collective-permute-start(bf16[4,384,256]{2,1,0:T(8,128)(2,1)S(1)} %bitcast.127), channel_id=1, source_target_pairs={{0,1},{1,0},{2,3},{3,2},{4,5},{5,4},{6,7},{7,6},{8,9},{9,8},{10,11... | collective-permute-start | bytes 2359304 | tf_op jit(solution)/shard_map/ppermute | solution.py:22
  272.3 3.6 %all-to-all-start.4 = ((f32[8,2,2,384]{3,2,1,0:T(2,128)}), f32[8,2,2,384]{3,2,1,0:T(2,128)S(1)}, u32[]{:S(2)}, u32[]{:S(2)}) async-start(f32[8,2,2,384]{3,2,1,0:T(2,128)} %broadcast_in_dim.61), calls=%async_computation.4 | async-start | bytes 98304 | tf_op jit(solution)/shard_map/all_to_all | solution.py:168
  275.9 4.8 %all-to-all-done.4 = f32[8,2,2,384]{3,2,1,0:T(2,128)S(1)} async-done(((f32[8,2,2,384]{3,2,1,0:T(2,128)}), f32[8,2,2,384]{3,2,1,0:T(2,128)S(1)}, u32[]{:S(2)}, u32[]{:S(2)}) %all-to-all-start.4) | async-done | bytes 49184 | tf_op jit(solution)/shard_map/all_to_all | solution.py:168
  (102 shorter events, 19.1 us)
Async XLA Ops:
  6.5 71.2 %slice-start = ((bf16[768,512]{1,0:T(8,128)(2,1)}), bf16[32,512]{1,0:T(8,128)(2,1)S(1)}, s32[]{:S(2)}) async-start(bf16[768,512]{1,0:T(8,128)(2,1)} %param.7), calls=%async_computation.6 | async-start | bytes 65536 | tf_op jit(solution)/shard_map/slice | solution.py:114
  6.5 80.7 %copy-start = (bf16[768,512]{1,0:T(8,128)(2,1)S(1)}, bf16[768,512]{1,0:T(8,128)(2,1)}, u32[]{:S(2)}) copy-start(bf16[768,512]{1,0:T(8,128)(2,1)} %param.7) | copy-start | bytes 2359300
  6.6 172.0 %all-gather.4.cloned.1.call-start = ((), (), s32[]{:S(2)}) async-start(), calls=%async_computation.5 | async-start | bytes 1671168 | tf_op jit(solution)/shard_map/all_gather | solution.py:92
  77.8 9.4 %collective-permute-start = (bf16[288,512]{1,0:T(8,128)(2,1)S(1)}, bf16[288,512]{1,0:T(8,128)(2,1)S(1)}, u32[]{:S(2)}, u32[]{:S(2)}) collective-permute-start(bf16[288,512]{1,0:T(8,128)(2,1)S(1)} %pad_maximum_fusion.3), channel_id=1, source_target_pairs={{0,8},{8,16},{16,24},{24,32},{32,40},{40,48},{48,56},{56,64},{64,7... | collective-permute-start | bytes 884744 | tf_op jit(solution)/shard_map/ppermute | solution.py:17
  82.5 7.1 %collective-permute-start.1 = (bf16[256,512]{1,0:T(8,128)(2,1)S(1)}, bf16[256,512]{1,0:T(8,128)(2,1)S(1)}, u32[]{:S(2)}, u32[]{:S(2)}) collective-permute-start(bf16[256,512]{1,0:T(8,128)(2,1)S(1)} %get-tuple-element.31), channel_id=1, source_target_pairs={{0,248},{8,0},{16,8},{24,16},{32,24},{40,32},{48,40},{56,48},{64,5... | collective-permute-start | bytes 786440 | tf_op jit(solution)/shard_map/ppermute | solution.py:17
  87.4 16.4 %copy-start.3 = (bf16[416,512]{1,0:T(8,128)(2,1)}, bf16[416,512]{1,0:T(8,128)(2,1)S(1)}, u32[]{:S(2)}) copy-start(bf16[416,512]{1,0:T(8,128)(2,1)S(1)} %get-tuple-element.28) | copy-start | bytes 1277956
  90.2 11.3 %copy-start.9 = (bf16[2,32,512]{2,1,0:T(8,128)(2,1)S(1)}, bf16[2,32,512]{2,1,0:T(8,128)(2,1)}, u32[]{:S(2)}) copy-start(bf16[2,32,512]{2,1,0:T(8,128)(2,1)} %param.9) | copy-start | bytes 196612
  91.8 12.0 %collective-permute-start.2 = (bf16[4,416,256]{2,1,0:T(8,128)(2,1)}, bf16[4,416,256]{2,1,0:T(8,128)(2,1)}, u32[]{:S(2)}, u32[]{:S(2)}) collective-permute-start(bf16[4,416,256]{2,1,0:T(8,128)(2,1)} %fusion.7), channel_id=1, source_target_pairs={{0,1},{1,0},{2,3},{3,2},{4,5},{5,4},{6,7},{7,6},{8,9},{9,8},{10,11... | collective-permute-start | bytes 2555912 | tf_op jit(solution)/shard_map/ppermute | solution.py:22
  106.5 4.8 %copy-start.10 = (f32[2,1024]{1,0:T(2,128)S(1)}, f32[2,1024]{1,0:T(2,128)}, u32[]{:S(2)}) copy-start(f32[2,1024]{1,0:T(2,128)} %param.11) | copy-start | bytes 24580
  106.5 4.9 %copy-start.1 = (bf16[2,4,256,256]{3,2,1,0:T(8,128)(2,1)S(1)}, bf16[2,4,256,256]{3,2,1,0:T(8,128)(2,1)}, u32[]{:S(2)}) copy-start(bf16[2,4,256,256]{3,2,1,0:T(8,128)(2,1)} %param.10) | copy-start | bytes 3145732
  106.5 17.2 %all-to-all-start = ((bf16[4,416,256]{2,1,0:T(8,128)(2,1)}), bf16[4,416,256]{2,1,0:T(8,128)(2,1)S(1)}, u32[]{:S(2)}, u32[]{:S(2)}) async-start(bf16[4,416,256]{2,1,0:T(8,128)(2,1)} %fusion), calls=%async_computation | async-start | bytes 1703936 | tf_op jit(solution)/shard_map/all_to_all | solution.py:36
  124.7 4.6 %copy-start.11 = (f32[2,512]{1,0:T(2,128)S(1)}, f32[2,512]{1,0:T(2,128)}, u32[]{:S(2)}) copy-start(f32[2,512]{1,0:T(2,128)} %param.12) | copy-start | bytes 12292
  125.6 14.7 %all-to-all-start.1 = ((bf16[4,400,256]{2,1,0:T(8,128)(2,1)}), bf16[4,400,256]{2,1,0:T(8,128)(2,1)S(1)}, u32[]{:S(2)}, u32[]{:S(2)}) async-start(bf16[4,400,256]{2,1,0:T(8,128)(2,1)} %broadcast_in_dim.55), calls=%async_computation.1 | async-start | bytes 1638400 | tf_op jit(solution)/shard_map/all_to_all | solution.py:36
  140.4 51.3 %collective-permute-start.3 = (bf16[4,400,256]{2,1,0:T(8,128)(2,1)S(1)}, bf16[4,400,256]{2,1,0:T(8,128)(2,1)}, u32[]{:S(2)}, u32[]{:S(2)}) collective-permute-start(bf16[4,400,256]{2,1,0:T(8,128)(2,1)S(1)} %all-to-all-done.1), channel_id=1, source_target_pairs={{0,1},{1,0},{2,3},{3,2},{4,5},{5,4},{6,7},{7,6},{8,9},{9,8},{10,11... | collective-permute-start | bytes 2457608 | tf_op jit(solution)/shard_map/ppermute | solution.py:22
  179.6 9.1 %collective-permute-start.4 = (bf16[256,512]{1,0:T(8,128)(2,1)S(1)}, bf16[256,512]{1,0:T(8,128)(2,1)S(1)}, u32[]{:S(2)}, u32[]{:S(2)}) collective-permute-start(bf16[256,512]{1,0:T(8,128)(2,1)S(1)} %get-tuple-element.24), channel_id=1, source_target_pairs={{0,8},{8,16},{16,24},{24,32},{32,40},{40,48},{48,56},{56,64},{64,7... | collective-permute-start | bytes 786440 | tf_op jit(solution)/shard_map/ppermute | solution.py:17
  182.1 8.2 %collective-permute-start.5 = (bf16[256,512]{1,0:T(8,128)(2,1)S(1)}, bf16[256,512]{1,0:T(8,128)(2,1)S(1)}, u32[]{:S(2)}, u32[]{:S(2)}) collective-permute-start(bf16[256,512]{1,0:T(8,128)(2,1)S(1)} %get-tuple-element.25), channel_id=1, source_target_pairs={{0,248},{8,0},{16,8},{24,16},{32,24},{40,32},{48,40},{56,48},{64,5... | collective-permute-start | bytes 786440 | tf_op jit(solution)/shard_map/ppermute | solution.py:17
  188.8 2.1 copy-start.4
  191.6 18.3 %copy-start.12 = (f32[2,512]{1,0:T(2,128)S(1)}, f32[2,512]{1,0:T(2,128)}, u32[]{:S(2)}) copy-start(f32[2,512]{1,0:T(2,128)} %param.13) | copy-start | bytes 12292
  194.2 20.5 %all-to-all-start.2 = ((f32[8,2,2,400]{3,2,1,0:T(2,128)}), f32[8,2,2,400]{3,2,1,0:T(2,128)S(1)}, u32[]{:S(2)}, u32[]{:S(2)}) async-start(f32[8,2,2,400]{3,2,1,0:T(2,128)} %broadcast_in_dim.56), calls=%async_computation.2 | async-start | bytes 131072 | tf_op jit(solution)/shard_map/all_to_all | solution.py:168
  209.9 15.6 %collective-permute-start.6 = (bf16[512,512]{1,0:T(8,128)(2,1)}, bf16[512,512]{1,0:T(8,128)(2,1)S(1)}, u32[]{:S(2)}, u32[]{:S(2)}) collective-permute-start(bf16[512,512]{1,0:T(8,128)(2,1)} %get-tuple-element.20), channel_id=1, source_target_pairs={{0,8},{8,0},{16,24},{24,16},{32,40},{40,32},{48,56},{56,48},{64,72... | collective-permute-start | bytes 1572872 | tf_op jit(solution)/shard_map/ppermute | solution.py:22
  215.2 11.5 %copy-start.5 = (bf16[400,512]{1,0:T(8,128)(2,1)}, bf16[400,512]{1,0:T(8,128)(2,1)S(1)}, u32[]{:S(2)}) copy-start(bf16[400,512]{1,0:T(8,128)(2,1)S(1)} %get-tuple-element.49) | copy-start | bytes 1228804
  215.2 16.2 %copy-start.7 = (bf16[400,512]{1,0:T(8,128)(2,1)}, bf16[400,512]{1,0:T(8,128)(2,1)S(1)}, u32[]{:S(2)}) copy-start(bf16[400,512]{1,0:T(8,128)(2,1)S(1)} %get-tuple-element.48) | copy-start | bytes 1228804
  226.6 4.8 %collective-permute-start.7 = (bf16[4,400,256]{2,1,0:T(8,128)(2,1)S(1)}, bf16[4,400,256]{2,1,0:T(8,128)(2,1)S(1)}, u32[]{:S(2)}, u32[]{:S(2)}) collective-permute-start(bf16[4,400,256]{2,1,0:T(8,128)(2,1)S(1)} %fusion.8), channel_id=1, source_target_pairs={{0,1},{1,0},{2,3},{3,2},{4,5},{5,4},{6,7},{7,6},{8,9},{9,8},{10,11... | collective-permute-start | bytes 2457608 | tf_op jit(solution)/shard_map/ppermute | solution.py:22
  232.9 4.4 %copy-start.2 = (bf16[512,512]{1,0:T(8,128)(2,1)S(1)}, bf16[512,512]{1,0:T(8,128)(2,1)}, u32[]{:S(2)}) copy-start(bf16[512,512]{1,0:T(8,128)(2,1)} %get-tuple-element.19) | copy-start | bytes 1572868
  232.9 16.4 %all-to-all-start.3 = ((bf16[4,400,256]{2,1,0:T(8,128)(2,1)}), bf16[4,400,256]{2,1,0:T(8,128)(2,1)S(1)}, u32[]{:S(2)}, u32[]{:S(2)}) async-start(bf16[4,400,256]{2,1,0:T(8,128)(2,1)} %fusion.1), calls=%async_computation.3 | async-start | bytes 1638400 | tf_op jit(solution)/shard_map/all_to_all | solution.py:36
  237.3 31.7 %collective-permute-start.9 = (bf16[512,512]{1,0:T(8,128)(2,1)S(1)}, bf16[512,512]{1,0:T(8,128)(2,1)S(1)}, u32[]{:S(2)}, u32[]{:S(2)}) collective-permute-start(bf16[512,512]{1,0:T(8,128)(2,1)S(1)} %copy-done.2), channel_id=1, source_target_pairs={{0,8},{8,0},{16,24},{24,16},{32,40},{40,32},{48,56},{56,48},{64,72... | collective-permute-start | bytes 1572872 | tf_op jit(solution)/shard_map/ppermute | solution.py:22
  251.1 18.4 %copy-start.8 = (bf16[400,512]{1,0:T(8,128)(2,1)S(1)}, bf16[400,512]{1,0:T(8,128)(2,1)}, u32[]{:S(2)}) copy-start(bf16[400,512]{1,0:T(8,128)(2,1)} %copy-done.7) | copy-start | bytes 1228804
  262.7 8.2 %collective-permute-start.8 = (bf16[4,384,256]{2,1,0:T(8,128)(2,1)S(1)}, bf16[4,384,256]{2,1,0:T(8,128)(2,1)S(1)}, u32[]{:S(2)}, u32[]{:S(2)}) collective-permute-start(bf16[4,384,256]{2,1,0:T(8,128)(2,1)S(1)} %bitcast.127), channel_id=1, source_target_pairs={{0,1},{1,0},{2,3},{3,2},{4,5},{5,4},{6,7},{7,6},{8,9},{9,8},{10,11... | collective-permute-start | bytes 2359304 | tf_op jit(solution)/shard_map/ppermute | solution.py:22
  269.5 1.4 copy-start.6
  272.3 8.5 %all-to-all-start.4 = ((f32[8,2,2,384]{3,2,1,0:T(2,128)}), f32[8,2,2,384]{3,2,1,0:T(2,128)S(1)}, u32[]{:S(2)}, u32[]{:S(2)}) async-start(f32[8,2,2,384]{3,2,1,0:T(2,128)} %broadcast_in_dim.61), calls=%async_computation.4 | async-start | bytes 98304 | tf_op jit(solution)/shard_map/all_to_all | solution.py:168
Sparse Core Ops, SparseCore 0:
  102.3 76.1 all-gather.3

commit v2 on v0

--- a/solution.py
+++ b/solution.py
@@ -89,8 +89,11 @@
     first_in = lax.all_gather(
         in_weight[0], "sp", axis=0, axis_index_groups=every_other(), tiled=True
     )
+    upper = lax.axis_index("grp") % 2 == 1
+    half = width // 2
+    last_half = chosen(upper, out_weight[1][:, half:], out_weight[1][:, :half])
     later = lax.all_gather(
-        jnp.concatenate([out_weight[0], in_weight[1], out_weight[1]], axis=1),
+        jnp.concatenate([out_weight[0], in_weight[1], last_half], axis=1),
         "sp",
         axis=0,
         axis_index_groups=every_other(),
@@ -128,7 +131,9 @@
         partial = chip_partial(kept, sent, whole_in)
         pieces = between_chips(partial)
         if layer_index == 1:
-            whole_out = from_partner(later[:, 2 * width :])
+            own_half = later[:, 2 * width :]
+            rows_here = ordered(own_half, paired_half, upper, 1)
+            whole_out = from_partner(rows_here)
         hidden = pieces.astype(jnp.float32).sum(axis=0).astype(jnp.bfloat16)
         pooled = pooled_windows(hidden, group, positions)[drop:]
         mixed = jnp.dot(
@@ -163,6 +168,7 @@
         other_sum, other_stats = layer_sum(other_rows, sent[drop:])
         if layer_index == 0:
             next_in = from_partner(later[:, width : 2 * width])
+            paired_half = swapped(later[:, 2 * width :], "grp")
         stats = jnp.stack([chosen(lower, own_stats, other_stats), chosen(lower, other_stats, own_stats)])
         count = lax.axis_size("tp")
         everyones = lax.all_to_all(
@@ -184,11 +190,12 @@
                 normed * norm_gain[layer_index][None, :] + norm_shift[layer_index][None, :]
             ).astype(jnp.bfloat16)
 
+        if layer_index == LAYERS - 1:
+            sums = ordered(own_sum, other_sum, core == 1, 0)
+            return normalised(sums, jnp.concatenate([totals[0], totals[1]], axis=1))
         kept = normalised(own_sum, own_totals)
         sent = normalised(other_sum, other_totals)
         whole_in = next_in
-
-    return ordered(kept, sent, core == 1, 0)
 
 
 def solution(mesh):

time: 290 us -> 280 us (0.966)
  waiting for transfers between devices: 94.2 us -> 77.3 us
  starting transfers between devices: 73.8 us -> 77.1 us
    all_to_all x3, waiting for transfers between devices: 31.9 us -> 22.5 us  [between_chips(): lax.all_to_all(x, 'tp', split_axis=0, concat_axis=0, axis_index_groups=ch...]
    ppermute x6 -> x7, waiting for transfers between devices: 14.3 us -> 9.65 us  [swapped(): return lax.ppermute(x, axis, [(i, i ^ 1) for i in range(n)])]
    ppermute x6 -> x7, starting transfers between devices: 28.5 us -> 31.6 us  [swapped(): return lax.ppermute(x, axis, [(i, i ^ 1) for i in range(n)])]
  transfers between devices with their start and end apart: 16 -> 17, of which waited for: 14 -> 10; matrix products, arithmetic and copies ran while one was open for 5% -> 7% of each run, Pallas kernels for 0% -> 0%
where the time goes in v2:
time: 280 us; the launch traced here: 279 us
  blocking collectives  82.3 us (29%)
  waiting for transfers between devices  77.3 us (28%)
  starting transfers between devices  77.1 us (28%)
  between operations  14.1 us (5%)
  matrix products  11.9 us (4%)
  local copies, waits for them, and re-layouts  9.28 us (3%)
  other arithmetic  7.14 us (3%)
    all_gather x1, blocking collectives, per_device(): lax.all_gather(in_weight[0], 'sp', axis=0, axis_index_groups=every_other(...  70.3 us
    all_gather x1, waiting for transfers between devices, per_device(): lax.all_gather(jnp.concatenate([out_weight[0], in_weight[1], last_half],...  32 us
    ppermute x7, starting transfers between devices, swapped(): return lax.ppermute(x, axis, [(i, i ^ 1) for i in range(n)])  31.6 us
    all_to_all x3, waiting for transfers between devices, between_chips(): lax.all_to_all(x, 'tp', split_axis=0, concat_axis=0, axis_index_groups=ch...  22.5 us
    all_to_all x2, starting transfers between devices, per_device(): lax.all_to_all(jnp.broadcast_to(stats, (count, *stats.shape)), 'tp', spli...  20.2 us
    ppermute x4, starting transfers between devices, shifted(): return lax.ppermute(x, axis, [(i, (i + distance) % n) for i in range(n)])  13.4 us
    all_gather x1, blocking collectives, per_device(): lax.all_gather(scaled[None], 'tp', axis=0, axis_index_groups=chips(), til...  12 us
    all_to_all x3, starting transfers between devices, between_chips(): lax.all_to_all(x, 'tp', split_axis=0, concat_axis=0, axis_index_groups=ch...  11.9 us
  transfers between devices with their start and end apart: 17, of which 10 were waited for; matrix products, arithmetic and copies ran while one was open for 7% of the time, Pallas kernels for 0%

profile of v2, /device:TPU:33, one launch (start us, length us, event | category | flops | bytes accessed | tf_op | source)
XLA Modules:
  0.0 279.2 jit_solution(18124892601996126362)
XLA Ops:
  7.3 70.3 %all-gather = bf16[1,512,512]{2,1,0:T(8,128)(2,1)S(1)} all-gather(bf16[1,32,512]{2,1,0:T(8,128)(2,1)S(1)} %get-tuple-element.29), channel_id=2, replica_groups={{0,16,32,48,64,80,96,112,128,144,160,176,192,208,224,240},{8,24,40,56,7..., dimensions={1}, use_global_device_ids=true | all-gather | bytes 557056 | tf_op jit(solution)/shard_map/all_gather | solution.py:89
  77.7 4.9 %collective-permute-start = (bf16[288,512]{1,0:T(8,128)(2,1)S(1)}, bf16[288,512]{1,0:T(8,128)(2,1)S(1)}, u32[]{:S(2)}, u32[]{:S(2)}) collective-permute-start(bf16[288,512]{1,0:T(8,128)(2,1)S(1)} %pad_maximum_fusion.3), channel_id=1, source_target_pairs={{0,8},{8,16},{16,24},{24,32},{32,40},{40,48},{48,56},{56,64},{64,7... | collective-permute-start | bytes 884744 | tf_op jit(solution)/shard_map/ppermute | solution.py:17
  82.6 2.0 collective-permute-start.1
  84.6 2.7 collective-permute-done
  87.5 2.3 collective-permute-done.1
  90.3 1.5 fusion.7
  91.9 9.7 %collective-permute-start.2 = (bf16[4,416,256]{2,1,0:T(8,128)(2,1)}, bf16[4,416,256]{2,1,0:T(8,128)(2,1)}, u32[]{:S(2)}, u32[]{:S(2)}) collective-permute-start(bf16[4,416,256]{2,1,0:T(8,128)(2,1)} %fusion.7), channel_id=1, source_target_pairs={{0,1},{1,0},{2,3},{3,2},{4,5},{5,4},{6,7},{7,6},{8,9},{9,8},{10,11... | collective-permute-start | bytes 2555912 | tf_op jit(solution)/shard_map/ppermute | solution.py:22
  103.9 2.7 fusion
  106.6 4.8 %all-to-all-start = ((bf16[4,416,256]{2,1,0:T(8,128)(2,1)}), bf16[4,416,256]{2,1,0:T(8,128)(2,1)S(1)}, u32[]{:S(2)}, u32[]{:S(2)}) async-start(bf16[4,416,256]{2,1,0:T(8,128)(2,1)} %fusion), calls=%async_computation | async-start | bytes 1703936 | tf_op jit(solution)/shard_map/all_to_all | solution.py:36
  112.4 11.5 %all-to-all-done = bf16[4,416,256]{2,1,0:T(8,128)(2,1)S(1)} async-done(((bf16[4,416,256]{2,1,0:T(8,128)(2,1)}), bf16[4,416,256]{2,1,0:T(8,128)(2,1)S(1)}, u32[]{:S(2)}, u32[]{:S(2)}) %all-to-all-start) | async-done | bytes 852000 | tf_op jit(solution)/shard_map/all_to_all | solution.py:36
  125.7 3.6 %all-to-all-start.1 = ((bf16[4,400,256]{2,1,0:T(8,128)(2,1)}), bf16[4,400,256]{2,1,0:T(8,128)(2,1)S(1)}, u32[]{:S(2)}, u32[]{:S(2)}) async-start(bf16[4,400,256]{2,1,0:T(8,128)(2,1)} %broadcast_in_dim.55), calls=%async_computation.1 | async-start | bytes 1638400 | tf_op jit(solution)/shard_map/all_to_all | solution.py:36
  129.4 11.1 %all-to-all-done.1 = bf16[4,400,256]{2,1,0:T(8,128)(2,1)S(1)} async-done(((bf16[4,400,256]{2,1,0:T(8,128)(2,1)}), bf16[4,400,256]{2,1,0:T(8,128)(2,1)S(1)}, u32[]{:S(2)}, u32[]{:S(2)}) %all-to-all-start.1) | async-done | bytes 819232 | tf_op jit(solution)/shard_map/all_to_all | solution.py:36
  140.5 4.3 %collective-permute-start.3 = (bf16[4,400,256]{2,1,0:T(8,128)(2,1)S(1)}, bf16[4,400,256]{2,1,0:T(8,128)(2,1)}, u32[]{:S(2)}, u32[]{:S(2)}) collective-permute-start(bf16[4,400,256]{2,1,0:T(8,128)(2,1)S(1)} %all-to-all-done.1), channel_id=1, source_target_pairs={{0,1},{1,0},{2,3},{3,2},{4,5},{5,4},{6,7},{7,6},{8,9},{9,8},{10,11... | collective-permute-start | bytes 2457608 | tf_op jit(solution)/shard_map/ppermute | solution.py:22
  144.8 32.0 %all-gather.4.cloned.1.call-done = bf16[512,1280]{1,0:T(8,128)(2,1)} async-done(((bf16[32,1280]{1,0:T(8,128)(2,1)}), bf16[512,1280]{1,0:T(8,128)(2,1)}) %all-gather.4.cloned.1.call-update) | async-done | bytes 1310736 | tf_op jit(solution)/shard_map/all_gather | solution.py:95
  177.9 2.0 collective-permute-start.4
  179.8 4.6 %collective-permute-start.5 = (bf16[256,512]{1,0:T(8,128)(2,1)S(1)}, bf16[256,512]{1,0:T(8,128)(2,1)S(1)}, u32[]{:S(2)}, u32[]{:S(2)}) collective-permute-start(bf16[256,512]{1,0:T(8,128)(2,1)S(1)} %get-tuple-element.20), channel_id=1, source_target_pairs={{0,248},{8,0},{16,8},{24,16},{32,24},{40,32},{48,40},{56,48},{64,5... | collective-permute-start | bytes 786440 | tf_op jit(solution)/shard_map/ppermute | solution.py:17
  185.7 2.0 collective-permute-start.6
  189.3 1.9 fusion.43
  191.8 16.7 %all-to-all-start.2 = ((f32[8,2,2,400]{3,2,1,0:T(2,128)}), f32[8,2,2,400]{3,2,1,0:T(2,128)S(1)}, u32[]{:S(2)}, u32[]{:S(2)}) async-start(f32[8,2,2,400]{3,2,1,0:T(2,128)} %broadcast_in_dim.56), calls=%async_computation.2 | async-start | bytes 131072 | tf_op jit(solution)/shard_map/all_to_all | solution.py:174
  208.5 1.6 maximum_select_fusion.3
  210.1 3.3 %all-to-all-done.2 = f32[8,2,2,400]{3,2,1,0:T(2,128)S(1)} async-done(((f32[8,2,2,400]{3,2,1,0:T(2,128)}), f32[8,2,2,400]{3,2,1,0:T(2,128)S(1)}, u32[]{:S(2)}, u32[]{:S(2)}) %all-to-all-start.2) | async-done | bytes 51232 | tf_op jit(solution)/shard_map/all_to_all | solution.py:174
  215.2 2.7 collective-permute-start.7
  217.9 1.9 collective-permute-done.7
  219.8 1.6 fusion.1
  221.4 3.6 %all-to-all-start.3 = ((bf16[4,400,256]{2,1,0:T(8,128)(2,1)}), bf16[4,400,256]{2,1,0:T(8,128)(2,1)S(1)}, u32[]{:S(2)}, u32[]{:S(2)}) async-start(bf16[4,400,256]{2,1,0:T(8,128)(2,1)} %fusion.1), calls=%async_computation.3 | async-start | bytes 1638400 | tf_op jit(solution)/shard_map/all_to_all | solution.py:36
  226.0 3.1 %collective-permute-start.9 = (bf16[512,256]{1,0:T(8,128)(2,1)S(1)}, bf16[512,256]{1,0:T(8,128)(2,1)S(1)}, u32[]{:S(2)}, u32[]{:S(2)}) collective-permute-start(bf16[512,256]{1,0:T(8,128)(2,1)S(1)} %slice.253), channel_id=1, source_target_pairs={{0,256},{256,0},{1,257},{257,1},{2,258},{258,2},{3,259},{259,3},{4... | collective-permute-start | bytes 786440 | tf_op jit(solution)/shard_map/ppermute | solution.py:22
  229.2 6.2 %collective-permute-done.9 = bf16[512,256]{1,0:T(8,128)(2,1)S(1)} collective-permute-done((bf16[512,256]{1,0:T(8,128)(2,1)S(1)}, bf16[512,256]{1,0:T(8,128)(2,1)S(1)}, u32[]{:S(2)}, u32[]{:S(2)}) %collective-permute-start.9) | collective-permute-done | bytes 262176 | tf_op jit(solution)/shard_map/ppermute | solution.py:22
  235.5 3.7 %collective-permute-start.10 = (bf16[512,512]{1,0:T(8,128)(2,1)S(1)}, bf16[512,512]{1,0:T(8,128)(2,1)S(1)}, u32[]{:S(2)}, u32[]{:S(2)}) collective-permute-start(bf16[512,512]{1,0:T(8,128)(2,1)S(1)} %maximum_select_fusion.5), channel_id=1, source_target_pairs={{0,8},{8,0},{16,24},{24,16},{32,40},{40,32},{48,56},{56,48},{64,72... | collective-permute-start | bytes 1572872 | tf_op jit(solution)/shard_map/ppermute | solution.py:22
  241.0 12.0 %all-gather.1 = bf16[1536,256]{1,0:T(8,128)(2,1)S(1)} all-gather(bf16[384,256]{1,0:T(8,128)(2,1)S(1)} %fusion.14), channel_id=3, replica_groups={{0,2,4,6},{1,3,5,7},{8,10,12,14},{9,11,13,15},{16,18,20,22},{17,19,21,2..., dimensions={0}, use_global_device_ids=true | all-gather | bytes 983040 | tf_op jit(solution)/shard_map/all_gather | solution.py:153
  253.0 6.1 %collective-permute-start.8 = (bf16[4,384,256]{2,1,0:T(8,128)(2,1)S(1)}, bf16[4,384,256]{2,1,0:T(8,128)(2,1)S(1)}, u32[]{:S(2)}, u32[]{:S(2)}) collective-permute-start(bf16[4,384,256]{2,1,0:T(8,128)(2,1)S(1)} %bitcast.127), channel_id=1, source_target_pairs={{0,1},{1,0},{2,3},{3,2},{4,5},{5,4},{6,7},{7,6},{8,9},{9,8},{10,11... | collective-permute-start | bytes 2359304 | tf_op jit(solution)/shard_map/ppermute | solution.py:22
  262.7 3.5 %all-to-all-start.4 = ((f32[8,2,2,384]{3,2,1,0:T(2,128)}), f32[8,2,2,384]{3,2,1,0:T(2,128)S(1)}, u32[]{:S(2)}, u32[]{:S(2)}) async-start(f32[8,2,2,384]{3,2,1,0:T(2,128)} %broadcast_in_dim.61), calls=%async_computation.4 | async-start | bytes 98304 | tf_op jit(solution)/shard_map/all_to_all | solution.py:174
  266.2 4.8 %all-to-all-done.4 = f32[8,2,2,384]{3,2,1,0:T(2,128)S(1)} async-done(((f32[8,2,2,384]{3,2,1,0:T(2,128)}), f32[8,2,2,384]{3,2,1,0:T(2,128)S(1)}, u32[]{:S(2)}, u32[]{:S(2)}) %all-to-all-start.4) | async-done | bytes 49184 | tf_op jit(solution)/shard_map/all_to_all | solution.py:174
  (107 shorter events, 20.7 us)
Async XLA Ops:
  6.5 71.1 %slice-start = ((bf16[768,512]{1,0:T(8,128)(2,1)}), bf16[32,512]{1,0:T(8,128)(2,1)S(1)}, s32[]{:S(2)}) async-start(bf16[768,512]{1,0:T(8,128)(2,1)} %param.7), calls=%async_computation.6 | async-start | bytes 65536 | tf_op jit(solution)/shard_map/slice | solution.py:117
  6.5 170.2 %all-gather.4.cloned.1.call-start = ((), (), s32[]{:S(2)}) async-start(), calls=%async_computation.5 | async-start | bytes 1392640 | tf_op jit(solution)/shard_map/all_gather | solution.py:95
  77.6 9.7 %copy-start = (bf16[768,512]{1,0:T(8,128)(2,1)S(1)}, bf16[768,512]{1,0:T(8,128)(2,1)}, u32[]{:S(2)}) copy-start(bf16[768,512]{1,0:T(8,128)(2,1)} %param.7) | copy-start | bytes 2359300
  77.7 9.5 %collective-permute-start = (bf16[288,512]{1,0:T(8,128)(2,1)S(1)}, bf16[288,512]{1,0:T(8,128)(2,1)S(1)}, u32[]{:S(2)}, u32[]{:S(2)}) collective-permute-start(bf16[288,512]{1,0:T(8,128)(2,1)S(1)} %pad_maximum_fusion.3), channel_id=1, source_target_pairs={{0,8},{8,16},{16,24},{24,32},{32,40},{40,48},{48,56},{56,64},{64,7... | collective-permute-start | bytes 884744 | tf_op jit(solution)/shard_map/ppermute | solution.py:17
  82.6 7.1 %collective-permute-start.1 = (bf16[256,512]{1,0:T(8,128)(2,1)S(1)}, bf16[256,512]{1,0:T(8,128)(2,1)S(1)}, u32[]{:S(2)}, u32[]{:S(2)}) collective-permute-start(bf16[256,512]{1,0:T(8,128)(2,1)S(1)} %get-tuple-element.28), channel_id=1, source_target_pairs={{0,248},{8,0},{16,8},{24,16},{32,24},{40,32},{48,40},{56,48},{64,5... | collective-permute-start | bytes 786440 | tf_op jit(solution)/shard_map/ppermute | solution.py:17
  87.5 2.8 %copy-start.2 = (bf16[416,512]{1,0:T(8,128)(2,1)}, bf16[416,512]{1,0:T(8,128)(2,1)S(1)}, u32[]{:S(2)}) copy-start(bf16[416,512]{1,0:T(8,128)(2,1)S(1)} %get-tuple-element.26) | copy-start | bytes 1277956
  90.3 11.3 %copy-start.8 = (bf16[2,32,512]{2,1,0:T(8,128)(2,1)S(1)}, bf16[2,32,512]{2,1,0:T(8,128)(2,1)}, u32[]{:S(2)}) copy-start(bf16[2,32,512]{2,1,0:T(8,128)(2,1)} %param.9) | copy-start | bytes 196612
  91.9 12.1 %collective-permute-start.2 = (bf16[4,416,256]{2,1,0:T(8,128)(2,1)}, bf16[4,416,256]{2,1,0:T(8,128)(2,1)}, u32[]{:S(2)}, u32[]{:S(2)}) collective-permute-start(bf16[4,416,256]{2,1,0:T(8,128)(2,1)} %fusion.7), channel_id=1, source_target_pairs={{0,1},{1,0},{2,3},{3,2},{4,5},{5,4},{6,7},{7,6},{8,9},{9,8},{10,11... | collective-permute-start | bytes 2555912 | tf_op jit(solution)/shard_map/ppermute | solution.py:22
  106.6 4.8 %copy-start.9 = (f32[2,1024]{1,0:T(2,128)S(1)}, f32[2,1024]{1,0:T(2,128)}, u32[]{:S(2)}) copy-start(f32[2,1024]{1,0:T(2,128)} %param.11) | copy-start | bytes 24580
  106.6 4.9 %copy-start.1 = (bf16[2,4,256,256]{3,2,1,0:T(8,128)(2,1)S(1)}, bf16[2,4,256,256]{3,2,1,0:T(8,128)(2,1)}, u32[]{:S(2)}) copy-start(bf16[2,4,256,256]{3,2,1,0:T(8,128)(2,1)} %param.10) | copy-start | bytes 3145732
  106.6 17.2 %all-to-all-start = ((bf16[4,416,256]{2,1,0:T(8,128)(2,1)}), bf16[4,416,256]{2,1,0:T(8,128)(2,1)S(1)}, u32[]{:S(2)}, u32[]{:S(2)}) async-start(bf16[4,416,256]{2,1,0:T(8,128)(2,1)} %fusion), calls=%async_computation | async-start | bytes 1703936 | tf_op jit(solution)/shard_map/all_to_all | solution.py:36
  124.7 4.6 %copy-start.10 = (f32[2,512]{1,0:T(2,128)S(1)}, f32[2,512]{1,0:T(2,128)}, u32[]{:S(2)}) copy-start(f32[2,512]{1,0:T(2,128)} %param.12) | copy-start | bytes 12292
  124.8 4.6 %copy-start.11 = (f32[2,512]{1,0:T(2,128)S(1)}, f32[2,512]{1,0:T(2,128)}, u32[]{:S(2)}) copy-start(f32[2,512]{1,0:T(2,128)} %param.13) | copy-start | bytes 12292
  125.7 14.7 %all-to-all-start.1 = ((bf16[4,400,256]{2,1,0:T(8,128)(2,1)}), bf16[4,400,256]{2,1,0:T(8,128)(2,1)S(1)}, u32[]{:S(2)}, u32[]{:S(2)}) async-start(bf16[4,400,256]{2,1,0:T(8,128)(2,1)} %broadcast_in_dim.55), calls=%async_computation.1 | async-start | bytes 1638400 | tf_op jit(solution)/shard_map/all_to_all | solution.py:36
  140.5 48.6 %collective-permute-start.3 = (bf16[4,400,256]{2,1,0:T(8,128)(2,1)S(1)}, bf16[4,400,256]{2,1,0:T(8,128)(2,1)}, u32[]{:S(2)}, u32[]{:S(2)}) collective-permute-start(bf16[4,400,256]{2,1,0:T(8,128)(2,1)S(1)} %all-to-all-done.1), channel_id=1, source_target_pairs={{0,1},{1,0},{2,3},{3,2},{4,5},{5,4},{6,7},{7,6},{8,9},{9,8},{10,11... | collective-permute-start | bytes 2457608 | tf_op jit(solution)/shard_map/ppermute | solution.py:22
  177.9 9.8 %collective-permute-start.4 = (bf16[256,512]{1,0:T(8,128)(2,1)S(1)}, bf16[256,512]{1,0:T(8,128)(2,1)S(1)}, u32[]{:S(2)}, u32[]{:S(2)}) collective-permute-start(bf16[256,512]{1,0:T(8,128)(2,1)S(1)} %get-tuple-element.19), channel_id=1, source_target_pairs={{0,8},{8,16},{16,24},{24,32},{32,40},{40,48},{48,56},{56,64},{64,7... | collective-permute-start | bytes 786440 | tf_op jit(solution)/shard_map/ppermute | solution.py:17
  179.8 7.9 %collective-permute-start.5 = (bf16[256,512]{1,0:T(8,128)(2,1)S(1)}, bf16[256,512]{1,0:T(8,128)(2,1)S(1)}, u32[]{:S(2)}, u32[]{:S(2)}) collective-permute-start(bf16[256,512]{1,0:T(8,128)(2,1)S(1)} %get-tuple-element.20), channel_id=1, source_target_pairs={{0,248},{8,0},{16,8},{24,16},{32,24},{40,32},{48,40},{56,48},{64,5... | collective-permute-start | bytes 786440 | tf_op jit(solution)/shard_map/ppermute | solution.py:17
  185.7 22.8 %collective-permute-start.6 = (bf16[512,512]{1,0:T(8,128)(2,1)S(1)}, bf16[512,512]{1,0:T(8,128)(2,1)}, u32[]{:S(2)}, u32[]{:S(2)}) collective-permute-start(bf16[512,512]{1,0:T(8,128)(2,1)S(1)} %get-tuple-element.22), channel_id=1, source_target_pairs={{0,8},{8,0},{16,24},{24,16},{32,40},{40,32},{48,56},{56,48},{64,72... | collective-permute-start | bytes 1572872 | tf_op jit(solution)/shard_map/ppermute | solution.py:22
  188.3 1.0 copy-start.3
  191.8 21.5 %all-to-all-start.2 = ((f32[8,2,2,400]{3,2,1,0:T(2,128)}), f32[8,2,2,400]{3,2,1,0:T(2,128)S(1)}, u32[]{:S(2)}, u32[]{:S(2)}) async-start(f32[8,2,2,400]{3,2,1,0:T(2,128)} %broadcast_in_dim.56), calls=%async_computation.2 | async-start | bytes 131072 | tf_op jit(solution)/shard_map/all_to_all | solution.py:174
  213.8 0.8 copy-start.4
  213.8 6.0 %copy-start.6 = (bf16[400,512]{1,0:T(8,128)(2,1)}, bf16[400,512]{1,0:T(8,128)(2,1)S(1)}, u32[]{:S(2)}) copy-start(bf16[400,512]{1,0:T(8,128)(2,1)S(1)} %get-tuple-element.47) | copy-start | bytes 1228804
  215.2 4.7 %collective-permute-start.7 = (bf16[4,400,256]{2,1,0:T(8,128)(2,1)S(1)}, bf16[4,400,256]{2,1,0:T(8,128)(2,1)S(1)}, u32[]{:S(2)}, u32[]{:S(2)}) collective-permute-start(bf16[4,400,256]{2,1,0:T(8,128)(2,1)S(1)} %fusion.8), channel_id=1, source_target_pairs={{0,1},{1,0},{2,3},{3,2},{4,5},{5,4},{6,7},{7,6},{8,9},{9,8},{10,11... | collective-permute-start | bytes 2457608 | tf_op jit(solution)/shard_map/ppermute | solution.py:22
  221.4 17.8 %all-to-all-start.3 = ((bf16[4,400,256]{2,1,0:T(8,128)(2,1)}), bf16[4,400,256]{2,1,0:T(8,128)(2,1)S(1)}, u32[]{:S(2)}, u32[]{:S(2)}) async-start(bf16[4,400,256]{2,1,0:T(8,128)(2,1)} %fusion.1), calls=%async_computation.3 | async-start | bytes 1638400 | tf_op jit(solution)/shard_map/all_to_all | solution.py:36
  226.0 9.4 %collective-permute-start.9 = (bf16[512,256]{1,0:T(8,128)(2,1)S(1)}, bf16[512,256]{1,0:T(8,128)(2,1)S(1)}, u32[]{:S(2)}, u32[]{:S(2)}) collective-permute-start(bf16[512,256]{1,0:T(8,128)(2,1)S(1)} %slice.253), channel_id=1, source_target_pairs={{0,256},{256,0},{1,257},{257,1},{2,258},{258,2},{3,259},{259,3},{4... | collective-permute-start | bytes 786440 | tf_op jit(solution)/shard_map/ppermute | solution.py:22
  235.5 23.8 %collective-permute-start.10 = (bf16[512,512]{1,0:T(8,128)(2,1)S(1)}, bf16[512,512]{1,0:T(8,128)(2,1)S(1)}, u32[]{:S(2)}, u32[]{:S(2)}) collective-permute-start(bf16[512,512]{1,0:T(8,128)(2,1)S(1)} %maximum_select_fusion.5), channel_id=1, source_target_pairs={{0,8},{8,0},{16,24},{24,16},{32,40},{40,32},{48,56},{56,48},{64,72... | collective-permute-start | bytes 1572872 | tf_op jit(solution)/shard_map/ppermute | solution.py:22
  253.0 8.0 %collective-permute-start.8 = (bf16[4,384,256]{2,1,0:T(8,128)(2,1)S(1)}, bf16[4,384,256]{2,1,0:T(8,128)(2,1)S(1)}, u32[]{:S(2)}, u32[]{:S(2)}) collective-permute-start(bf16[4,384,256]{2,1,0:T(8,128)(2,1)S(1)} %bitcast.127), channel_id=1, source_target_pairs={{0,1},{1,0},{2,3},{3,2},{4,5},{5,4},{6,7},{7,6},{8,9},{9,8},{10,11... | collective-permute-start | bytes 2359304 | tf_op jit(solution)/shard_map/ppermute | solution.py:22
  259.3 1.0 copy-start.7
  260.3 1.0 copy-start.5
  262.7 8.3 %all-to-all-start.4 = ((f32[8,2,2,384]{3,2,1,0:T(2,128)}), f32[8,2,2,384]{3,2,1,0:T(2,128)S(1)}, u32[]{:S(2)}, u32[]{:S(2)}) async-start(f32[8,2,2,384]{3,2,1,0:T(2,128)} %broadcast_in_dim.61), calls=%async_computation.4 | async-start | bytes 98304 | tf_op jit(solution)/shard_map/all_to_all | solution.py:174
Sparse Core Ops, SparseCore 0:
  102.5 74.2 all-gather.3
